TPU v7x, 256 devices: a whole 4x4x8 slice. The times are simulated.
256 devices in a mesh: sp: 16 (over y, x), dp: 16 (over z, core).
Axes of the slice: x: 4, y: 4, z: 8, core: 2. Of those that a mesh axis runs over, the one named last changes fastest.
Arguments:
- tokens: bfloat16 [16, 6144, 2048], P('dp', 'sp'), may hold values from -6 to 6
- value_act: bfloat16 [16, 6144, 1024], P('dp', 'sp'), may hold values from -6 to 6
- gate_act: bfloat16 [16, 6144, 1024], P('dp', 'sp'), may hold values from -6 to 6
- cotangent: bfloat16 [16, 6144, 1024], P('dp', 'sp'), may hold values from -6 to 6
- value_weight: bfloat16 [2048, 1024], P('dp'), may hold values from -0.1875 to 0.1875
- gate_weight: bfloat16 [2048, 1024], P('dp'), may hold values from -0.1875 to 0.1875
- norm_gain: float32 [1024], replicated, may hold values from 0.1 to 1.9
- norm_bias: float32 [1024], replicated, may hold values from -3 to 3
- mix_weight: bfloat16 [16, 128, 128], replicated, may hold values from -0.5 to 0.5
- mix_bias: float32 [16, 128], replicated, may hold values from 0.1 to 1.9
Outputs:
- tokens_grad: bfloat16 [16, 6144, 2048], P('dp', 'sp')
- value_weight_grad: float32 [2048, 1024], P('dp')
- gate_weight_grad: float32 [2048, 1024], P('dp')
- mix_weight_grad: float32 [16, 128, 128], replicated
- mix_bias_grad: float32 [16, 128], replicated
- norm_gain_grad: float32 [1024], replicated
- norm_bias_grad: float32 [1024], replicated
All inputs are finite; a program needn't handle non-finite values.
Results may differ from a plain program's by a relative error of at most 0.0054.
Values may be sent and summed in bfloat16 or wider, within the bound.
A program may use at most 128 MiB of HBM per device.

v0:
```python
import jax
import jax.numpy as jnp
from jax import lax
from jax.sharding import PartitionSpec as P

EPSILON = 1e-06


def gelu_slope(values):
    cdf_part = 0.5 * (1.0 + lax.erf(values * 0.7071067811865476))
    pdf_part = jnp.exp(-0.5 * values * values) * 0.3989422804014327
    return cdf_part + values * pdf_part


def mixer_backward(value_act, gate_act, cotangent, norm_gain, norm_bias, mix_weight, mix_bias):
    seq_len, channels = value_act.shape
    groups, block_len = (mix_weight.shape[0], mix_weight.shape[1])
    group_dim = channels // groups
    blocks = seq_len // block_len
    value_float = value_act.astype(jnp.float32)
    gate_float = gate_act.astype(jnp.float32)
    activated = jax.nn.gelu(value_float, approximate=False)
    gate_gelu = jax.nn.gelu(gate_float, approximate=False)
    centred = gate_gelu - jnp.mean(gate_gelu, axis=-1, keepdims=True)
    inv_std = lax.rsqrt(jnp.mean(centred * centred, axis=-1, keepdims=True) + EPSILON)
    normed = centred * inv_std
    spread_in = (normed * norm_gain + norm_bias).astype(jnp.bfloat16)
    spread_in = spread_in.reshape(blocks, block_len, groups, group_dim)
    causal = jnp.tril(jnp.ones((block_len, block_len), dtype=bool))
    masked_weight = jnp.where(causal[None], mix_weight, jnp.zeros_like(mix_weight))
    spatial = jnp.einsum(
        "gts,bsgd->btgd", masked_weight, spread_in, preferred_element_type=jnp.float32
    )
    spatial = (spatial + mix_bias.T[None, :, :, None]).reshape(seq_len, channels)
    grad_out = cotangent.astype(jnp.float32)
    grad_act = grad_out * spatial
    grad_spatial = grad_out * activated
    grad_split = grad_spatial.reshape(blocks, block_len, groups, group_dim)
    bias_grad = jnp.sum(grad_split, axis=(0, 3)).T
    spatial_low = grad_split.astype(jnp.bfloat16)
    weight_grad = jnp.einsum(
        "btgd,bsgd->gts", spatial_low, spread_in, preferred_element_type=jnp.float32
    )
    weight_grad = jnp.where(causal[None], weight_grad, jnp.zeros_like(weight_grad))
    grad_norm = jnp.einsum(
        "gts,btgd->bsgd", masked_weight, spatial_low, preferred_element_type=jnp.float32
    )
    grad_norm = grad_norm.reshape(seq_len, channels)
    gain_grad = jnp.sum(grad_norm * normed, axis=0)
    shift_grad = jnp.sum(grad_norm, axis=0)
    grad_hat = grad_norm * norm_gain
    grad_gate = inv_std * (
        grad_hat
        - jnp.mean(grad_hat, axis=-1, keepdims=True)
        - normed * jnp.mean(grad_hat * normed, axis=-1, keepdims=True)
    )
    value_grad = (grad_act * gelu_slope(value_float)).astype(jnp.bfloat16)
    gate_grad = (grad_gate * gelu_slope(gate_float)).astype(jnp.bfloat16)
    return (value_grad, gate_grad, (weight_grad, bias_grad, gain_grad, shift_grad))


def shards(
    tokens,
    value_act,
    gate_act,
    cotangent,
    value_weight,
    gate_weight,
    norm_gain,
    norm_bias,
    mix_weight,
    mix_bias,
):
    value_grad, gate_grad, stats = mixer_backward(
        value_act[0], gate_act[0], cotangent[0], norm_gain, norm_bias, mix_weight, mix_bias
    )
    channels = value_grad.shape[1]
    both_grads = jnp.concatenate((value_grad, gate_grad), axis=1)
    both_weights = jnp.concatenate((value_weight, gate_weight), axis=1)
    input_grad = lax.dot_general(
        both_grads,
        lax.all_gather(both_weights, "dp", axis=0, tiled=True),
        (((1,), (1,)), ((), ())),
        preferred_element_type=jnp.float32,
    ).astype(jnp.bfloat16)
    inputs = tokens[0]
    shard_terms = lax.psum_scatter(
        lax.dot_general(
            inputs, both_grads, (((0,), (0,)), ((), ())), preferred_element_type=jnp.float32
        ),
        "dp",
        scatter_dimension=0,
        tiled=True,
    )
    weight_sums = lax.psum(shard_terms, "sp")
    totals = lax.psum((stats[0], stats[1], stats[2], stats[3]), ("sp", "dp"))
    return (
        input_grad[None],
        weight_sums[:, :channels],
        weight_sums[:, channels:],
        totals[0],
        totals[1],
        totals[2],
        totals[3],
    )


def solution(mesh):
    placed = (
        P("dp", "sp", None),
        P("dp", "sp", None),
        P("dp", "sp", None),
        P("dp", "sp", None),
        P("dp", None),
        P("dp", None),
        P(),
        P(),
        P(),
        P(),
    )
    return jax.shard_map(
        shards,
        mesh=mesh,
        in_specs=placed,
        out_specs=(P("dp", "sp", None), P("dp", None), P("dp", None), P(), P(), P(), P()),
        check_vma=False,
    )
```

profile of v0, /device:TPU:2, one launch (start us, length us, event | category | flops | bytes accessed | tf_op | source)
XLA Modules:
  0.0 603.1 jit_solution(7592910926025882119)
XLA Ops:
  7.2 0.0 copy-start
  7.2 0.0 reduce-scatter.2.cloned.1.call-start
  7.2 2.4 copy.20
  9.6 4.5 fusion.96
  14.2 0.0 copy-done.1
  14.2 0.0 copy-start.14
  14.2 0.0 copy-start.16
  14.2 1.9 convert_multiply_fusion.1
  16.1 0.0 copy-done.14
  16.1 0.1 mul.187
  16.1 0.0 copy-done.16
  16.1 0.1 add.58
  16.2 2.3 copy.28
  18.5 2.3 copy.19
  20.9 0.2 multiply_reduce_fusion.2
  21.1 3.4 reshape.153
  24.6 3.0 convert_multiply_fusion
  27.6 3.6 mul.200
  31.1 3.6 mul.202
  34.7 3.6 mul.177
  38.3 3.6 mul.179
  41.9 5.6 fusion.93
  47.6 0.0 copy-start.9
  47.6 0.0 copy-done.10
  47.6 0.0 copy-done.11
  47.6 0.0 copy-done.12
  47.6 0.0 copy-start.15
  47.6 4.0 multiply_reduce_fusion
  51.6 0.0 copy-start.5
  51.7 1.1 copy-done.5
  52.8 0.5 bitcast_add_fusion
  53.4 1.1 copy.27
  54.5 0.0 copy-done.3
  54.5 0.2 copy-done.4
  54.7 0.8 fusion.78
  55.5 0.0 copy-start.2
  55.5 1.1 copy.36
  56.7 0.3 copy-done.2
  56.9 1.5 fusion.79
  58.5 0.9 copy-done.8
  59.4 0.0 copy-done
  59.4 9.4 %convolution_bitcast_fusion = f32[2048,2048]{0,1:T(8,128)} fusion(bf16[1,384,2048]{2,1,0:T(8,128)(2,1)S(1)} %copy-done, bf16[384,1024]{0,1:T(8,128)(2,1)S(1)} %fusion.79, bf16[384,1024]{0,1:T(8,128)(2,1)S(1)} %fusion.78), kind=kOutput, calls=%fused_computation | convolution fusion | flops 3224371200 | bytes 19922944 | tf_op jit(solution)/shard_map/dot_general | solution.py:88
  68.7 0.0 reduce-scatter.2.cloned.1.call-update
  68.8 0.0 copy-start.6
  68.8 0.0 all-gather.2.cloned.1.call-start
  68.8 0.9 copy-done.13
  69.7 1.8 pad_maximum_fusion.3
  71.5 0.0 all-gather.2.cloned.1.call-update
  71.5 0.0 all-reduce.4.cloned.1.call-start
  71.5 100.9 %reduce-scatter.2.cloned.1.call-done = f32[128,2048]{0,1:T(8,128)} async-done(((f32[2048,2048]{0,1:T(8,128)}), f32[128,2048]{0,1:T(8,128)}) %reduce-scatter.2.cloned.1.call-update) | async-done | bytes 1048592 | tf_op jit(solution)/shard_map/reduce_scatter | solution.py:87
  172.4 0.0 all-reduce.4.cloned.1.call-update
  172.4 0.3 all-reduce.6.cloned.1.call-start
  172.7 2.9 fusion.80
  175.6 0.0 all-reduce.6.cloned.1.call-update
  175.6 0.1 reduce_sum.73
  175.7 0.1 reduce_sum.75
  175.8 77.8 %all-reduce = (f32[16,128]{1,0:T(8,128)}, f32[1024]{0:T(1024)}, f32[1024]{0:T(1024)}) all-reduce(f32[16,128]{1,0:T(8,128)S(1)} %bitcast.235, f32[1024]{0:T(1024)S(1)} %reduce_sum.73, f32[1024]{0:T(1024)S(1)} %reduce_sum.75), channel_id=1, replica_groups=mesh['sp'=16,'dp'=16] {'sp','dp'}, use_global_device_ids=true, to_apply=%region_8.9 | all-reduce | flops 4096 | bytes 32768 | tf_op jit(solution)/shard_map/psum | solution.py:96
  253.6 8.6 %fusion = bf16[1,384,2048]{2,1,0:T(8,128)(2,1)} fusion(bf16[2048,2048]{1,0:T(8,128)(2,1)} %all-gather.2.cloned.1.call-done, bf16[384,1024]{0,1:T(8,128)(2,1)} %copy-done.8, bf16[384,1024]{0,1:T(8,128)(2,1)} %copy-done.7), kind=kOutput, calls=%fused_computation.2 | convolution fusion | flops 3225157632 | bytes 11534336 | tf_op jit(solution)/shard_map/dot_general | solution.py:80
  262.2 67.5 %all-reduce.4.cloned.1.call-done = f32[128,2048]{0,1:T(8,128)} async-done(((f32[128,2048]{0,1:T(8,128)}), f32[128,2048]{0,1:T(8,128)}) %all-reduce.4.cloned.1.call-update) | async-done | bytes 1048592 | tf_op jit(solution)/shard_map/psum | solution.py:95
  329.6 1.3 fusion.98
  330.9 1.0 copy.38
  331.9 1.0 copy.37
  332.9 261.4 %all-reduce.6.cloned.1.call-done = f32[16,128,128]{2,1,0:T(8,128)} async-done(((f32[16,128,128]{2,1,0:T(8,128)}), f32[16,128,128]{2,1,0:T(8,128)}) %all-reduce.6.cloned.1.call-update) | async-done | bytes 1048592 | tf_op jit(solution)/shard_map/psum | solution.py:96
  594.3 2.3 copy.61
  (18 shorter events, 0.1 us)
Async XLA Ops:
  7.2 52.2 %copy-start = (bf16[1,384,2048]{2,1,0:T(8,128)(2,1)S(1)}, bf16[1,384,2048]{2,1,0:T(8,128)(2,1)}, u32[]{:S(2)}) copy-start(bf16[1,384,2048]{2,1,0:T(8,128)(2,1)} %param.10) | copy-start | bytes 4718596
  7.2 165.2 %reduce-scatter.2.cloned.1.call-start = ((), (), s32[]{:S(2)}) async-start(), calls=%async_computation.2 | async-start | bytes 17825792 | tf_op jit(solution)/shard_map/reduce_scatter | solution.py:87
  9.6 4.5 copy-start.1
  14.2 1.9 copy-start.14
  14.2 2.0 copy-start.16
  41.9 5.6 copy-start.10
  41.9 5.6 copy-start.11
  41.9 5.7 copy-start.12
  47.6 4.1 copy-start.9
  47.6 5.2 copy-start.15
  51.6 1.1 copy-start.5
  53.3 1.1 copy-start.3
  53.3 1.4 copy-start.4
  55.5 2.9 copy-start.7
  55.5 1.4 copy-start.2
  58.4 0.9 copy-start.8
  68.7 0.9 copy-start.13
  68.8 103.9 %copy-start.6 = (f32[3,128,16,64]{1,3,0,2:T(8,128)S(1)}, f32[3,128,16,64]{1,3,0,2:T(8,128)}, u32[]{:S(2)}) copy-start(f32[3,128,16,64]{1,3,0,2:T(8,128)} %copy-done.5) | copy-start | bytes 4718596
  68.8 184.8 %all-gather.2.cloned.1.call-start = ((), (), s32[]{:S(2)}) async-start(), calls=%async_computation.1 | async-start | bytes 8912896 | tf_op jit(solution)/shard_map/all_gather | solution.py:82
  71.5 258.2 %all-reduce.4.cloned.1.call-start = ((), (), s32[]{:S(2)}) async-start(), calls=%async_computation.3 | async-start | bytes 2097152 | tf_op jit(solution)/shard_map/psum | solution.py:95
  172.4 421.8 %all-reduce.6.cloned.1.call-start = ((), (), s32[]{:S(2)}) async-start(), calls=%async_computation.4 | async-start | bytes 2097152 | tf_op jit(solution)/shard_map/psum | solution.py:96
Sparse Core Ops, SparseCore 0:
  68.9 103.4 reduce-scatter.1
  174.8 55.9 all-gather.1
  234.0 95.5 all-reduce.3
  335.5 258.7 all-reduce.5
where the time goes:
time: 604 us; the launch traced here: 603 us
  waiting for transfers between devices  430 us (71%)
  blocking collectives  77.8 us (13%)
  local copies, waits for them, and re-layouts  36.4 us (6%)
  matrix products  25.4 us (4%)
  other arithmetic  19.3 us (3%)
  between operations  14 us (2%)
    psum x1, waiting for transfers between devices, shards(): totals = lax.psum((stats[0], stats[1], stats[2], stats[3]), ('sp', 'dp'))  261 us
    reduce_scatter x1, waiting for transfers between devices, shards(): lax.psum_scatter(lax.dot_general(inputs, both_grads, (((0,), (0,)), ((),...  101 us
    psum x1, blocking collectives, shards(): totals = lax.psum((stats[0], stats[1], stats[2], stats[3]), ('sp', 'dp'))  77.8 us
    psum x1, waiting for transfers between devices, shards(): weight_sums = lax.psum(shard_terms, 'sp')  67.5 us
    unnamed x40, local copies, waits for them, and re-layouts  14.9 us
  transfers between devices with their start and end apart: 4, of which 3 were waited for; matrix products, arithmetic and copies ran while one was open for 3% of the time, Pallas kernels for 0%

commit v1 on v0

--- a/solution.py
+++ b/solution.py
@@ -92,7 +92,11 @@
         scatter_dimension=0,
         tiled=True,
     )
-    weight_sums = lax.psum(shard_terms, "sp")
+    weight_sums = shard_terms
+    for hop in (1, 2, 4, 8):
+        weight_sums = weight_sums + lax.ppermute(
+            weight_sums, "sp", [(dev, dev ^ hop) for dev in range(16)]
+        )
     totals = lax.psum((stats[0], stats[1], stats[2], stats[3]), ("sp", "dp"))
     return (
         input_grad[None],

time: 604 us -> 498 us (0.82)
  waiting for transfers between devices: 430 us -> 304 us
  blocking collectives: 77.8 us -> 89.4 us
  starting transfers between devices: 0.38 us -> 6.8 us
    psum x1, waiting for transfers between devices: 261 us -> 141 us  [shards(): totals = lax.psum((stats[0], stats[1], stats[2], stats[3]), ('sp', 'dp'))]
    psum x1 -> x0, waiting for transfers between devices: 67.5 us -> none  [shards(): weight_sums = lax.psum(shard_terms, 'sp')]
    ppermute x0 -> x4, waiting for transfers between devices: none -> 61.6 us  [shards(): lax.ppermute(weight_sums, 'sp', [(dev, dev ^ hop) for dev in range(16)])]
    psum x1, blocking collectives: 77.8 us -> 89.4 us  [shards(): totals = lax.psum((stats[0], stats[1], stats[2], stats[3]), ('sp', 'dp'))]
    ppermute x0 -> x4, starting transfers between devices: none -> 6.68 us  [shards(): lax.ppermute(weight_sums, 'sp', [(dev, dev ^ hop) for dev in range(16)])]
    unnamed x40 -> x48, local copies, waits for them, and re-layouts: 14.9 us -> 15 us
  transfers between devices with their start and end apart: 4 -> 7, of which waited for: 3 -> 5; matrix products, arithmetic and copies ran while one was open for 3% -> 3% of each run, Pallas kernels for 0% -> 0%
where the time goes in v1:
time: 498 us; the launch traced here: 497 us
  waiting for transfers between devices  304 us (61%)
  blocking collectives  89.4 us (18%)
  local copies, waits for them, and re-layouts  35.3 us (7%)
  matrix products  24 us (5%)
  other arithmetic  21.4 us (4%)
  between operations  15.7 us (3%)
  starting transfers between devices  6.8 us (1%)
    psum x1, waiting for transfers between devices, shards(): totals = lax.psum((stats[0], stats[1], stats[2], stats[3]), ('sp', 'dp'))  141 us
    reduce_scatter x1, waiting for transfers between devices, shards(): lax.psum_scatter(lax.dot_general(inputs, both_grads, (((0,), (0,)), ((),...  102 us
    psum x1, blocking collectives, shards(): totals = lax.psum((stats[0], stats[1], stats[2], stats[3]), ('sp', 'dp'))  89.4 us
    ppermute x4, waiting for transfers between devices, shards(): lax.ppermute(weight_sums, 'sp', [(dev, dev ^ hop) for dev in range(16)])  61.6 us
    unnamed x48, local copies, waits for them, and re-layouts  15 us
  transfers between devices with their start and end apart: 7, of which 5 were waited for; matrix products, arithmetic and copies ran while one was open for 3% of the time, Pallas kernels for 0%

profile of v1, /device:TPU:2, one launch (start us, length us, event | category | flops | bytes accessed | tf_op | source)
XLA Modules:
  0.0 497.2 jit_solution(16014844902752506183)
XLA Ops:
  8.0 0.0 copy-start
  8.0 0.0 reduce-scatter.2.cloned.1.call-start
  8.1 2.4 copy.20
  10.5 4.5 fusion.96
  15.0 0.0 copy-start.18
  15.0 0.0 copy-start.20
  15.0 1.9 convert_multiply_fusion.1
  16.9 0.1 mul.187
  17.0 0.1 add.68
  17.1 2.3 copy.28
  19.4 2.4 copy.19
  21.7 0.2 multiply_reduce_fusion.2
  22.0 3.4 reshape.153
  25.4 3.0 convert_multiply_fusion
  28.4 3.6 mul.200
  32.0 3.6 mul.202
  35.6 3.6 mul.177
  39.2 3.6 mul.179
  42.8 5.6 %fusion.93 = (f32[128,16]{0,1:T(8,128)S(1)}, bf16[3,128,16,64]{1,3,0,2:T(8,128)(2,1)S(1)}) fusion(f32[3,128,16,64]{1,0,3,2:T(4,128)} %mul.202, f32[3,128,16,64]{1,0,3,2:T(4,128)} %mul.200, f32[3,128,16,64]{1,0,3,2:T(4,128)} %reshape.153), kind=kLoop, calls=%fused_computation.137 | loop fusion | flops 25163776 | bytes 5513216 | tf_op jit(solution)/shard_map/reduce_sum | solution.py:39
  48.5 0.0 copy-start.19
  48.5 4.0 multiply_reduce_fusion
  52.6 0.0 copy-start.6
  52.6 1.1 copy-done.6
  53.7 0.5 bitcast_add_fusion
  54.3 1.1 copy.27
  55.4 0.0 copy-done.4
  55.4 0.2 copy-done.5
  55.6 0.8 fusion.78
  56.5 1.1 copy.36
  57.6 0.3 copy-done.3
  57.9 1.5 fusion.79
  59.4 0.9 copy-done.10
  60.2 9.4 %convolution_bitcast_fusion = f32[2048,2048]{0,1:T(8,128)} fusion(bf16[1,384,2048]{2,1,0:T(8,128)(2,1)S(1)} %copy-done, bf16[384,1024]{0,1:T(8,128)(2,1)S(1)} %fusion.79, bf16[384,1024]{0,1:T(8,128)(2,1)S(1)} %fusion.78), kind=kOutput, calls=%fused_computation | convolution fusion | flops 3224371200 | bytes 19922944 | tf_op jit(solution)/shard_map/dot_general | solution.py:88
  69.6 0.0 reduce-scatter.2.cloned.1.call-update
  69.6 0.0 all-gather.2.cloned.1.call-start
  69.7 0.9 copy-done.16
  70.6 0.1 copy-done.17
  70.7 0.8 pad_maximum_fusion.3
  71.5 0.0 all-gather.2.cloned.1.call-update
  71.5 0.0 all-reduce.3.cloned.1.call-start
  71.6 101.7 %reduce-scatter.2.cloned.1.call-done = f32[128,2048]{0,1:T(8,128)} async-done(((f32[2048,2048]{0,1:T(8,128)}), f32[128,2048]{0,1:T(8,128)}) %reduce-scatter.2.cloned.1.call-update) | async-done | bytes 1048592 | tf_op jit(solution)/shard_map/reduce_scatter | solution.py:87
  173.3 0.5 collective-permute-start
  173.8 23.5 %collective-permute-done = f32[128,2048]{0,1:T(8,128)S(1)} collective-permute-done((f32[128,2048]{0,1:T(8,128)}, f32[128,2048]{0,1:T(8,128)S(1)}, u32[]{:S(2)}, u32[]{:S(2)}) %collective-permute-start) | collective-permute-done | bytes 1048608 | tf_op jit(solution)/shard_map/ppermute | solution.py:97
  197.4 1.4 add.77
  198.7 0.0 copy-start.7
  198.7 2.4 collective-permute-start.1
  201.1 22.5 %collective-permute-done.1 = f32[128,2048]{0,1:T(8,128)S(1)} collective-permute-done((f32[128,2048]{0,1:T(8,128)S(1)}, f32[128,2048]{0,1:T(8,128)S(1)}, u32[]{:S(2)}, u32[]{:S(2)}) %collective-permute-start.1) | collective-permute-done | bytes 1048608 | tf_op jit(solution)/shard_map/ppermute | solution.py:97
  223.6 0.1 add.78
  223.7 1.6 collective-permute-start.2
  225.3 1.8 fusion.80
  227.1 0.0 all-reduce.3.cloned.1.call-update
  227.1 0.1 reduce_sum.73
  227.2 0.1 reduce_sum.75
  227.3 89.4 %all-reduce = (f32[16,128]{1,0:T(8,128)}, f32[1024]{0:T(1024)}, f32[1024]{0:T(1024)}) all-reduce(f32[16,128]{1,0:T(8,128)S(1)} %bitcast.235, f32[1024]{0:T(1024)S(1)} %reduce_sum.73, f32[1024]{0:T(1024)S(1)} %reduce_sum.75), channel_id=1, replica_groups=mesh['sp'=16,'dp'=16] {'sp','dp'}, use_global_device_ids=true, to_apply=%region_7.8 | all-reduce | flops 4096 | bytes 32768 | tf_op jit(solution)/shard_map/psum | solution.py:100
  316.7 1.4 add.79
  318.1 2.2 collective-permute-start.3
  320.3 8.3 %fusion = bf16[1,384,2048]{2,1,0:T(8,128)(2,1)} fusion(bf16[2048,2048]{1,0:T(8,128)(2,1)} %all-gather.2.cloned.1.call-done, bf16[384,1024]{0,1:T(8,128)(2,1)} %copy-done.10, bf16[384,1024]{0,1:T(8,128)(2,1)S(1)} %copy-done.9), kind=kOutput, calls=%fused_computation.2 | convolution fusion | flops 3225157632 | bytes 11534336 | tf_op jit(solution)/shard_map/dot_general | solution.py:80
  328.6 15.6 %collective-permute-done.3 = f32[128,2048]{0,1:T(8,128)S(1)} collective-permute-done((f32[128,2048]{0,1:T(8,128)S(1)}, f32[128,2048]{0,1:T(8,128)S(1)}, u32[]{:S(2)}, u32[]{:S(2)}) %collective-permute-start.3) | collective-permute-done | bytes 1048608 | tf_op jit(solution)/shard_map/ppermute | solution.py:97
  344.2 0.1 add.80
  344.3 0.1 fusion.98
  344.4 1.0 copy.38
  345.4 1.0 copy.37
  346.4 141.1 %all-reduce.3.cloned.1.call-done = f32[16,128,128]{2,1,0:T(8,128)} async-done(((f32[16,128,128]{2,1,0:T(8,128)}), f32[16,128,128]{2,1,0:T(8,128)}) %all-reduce.3.cloned.1.call-update) | async-done | bytes 1048592 | tf_op jit(solution)/shard_map/psum | solution.py:100
  487.5 2.3 copy.60
  (35 shorter events, 0.1 us)
Async XLA Ops:
  8.0 52.2 %copy-start = (bf16[1,384,2048]{2,1,0:T(8,128)(2,1)S(1)}, bf16[1,384,2048]{2,1,0:T(8,128)(2,1)}, u32[]{:S(2)}) copy-start(bf16[1,384,2048]{2,1,0:T(8,128)(2,1)} %param.10) | copy-start | bytes 4718596
  8.0 165.3 %reduce-scatter.2.cloned.1.call-start = ((), (), s32[]{:S(2)}) async-start(), calls=%async_computation.2 | async-start | bytes 17825792 | tf_op jit(solution)/shard_map/reduce_scatter | solution.py:87
  10.5 4.5 copy-start.2
  15.0 1.9 copy-start.18
  15.0 2.0 copy-start.20
  42.8 5.6 %copy-start.13 = (f32[3,128,16,64]{1,0,3,2:T(4,128)S(1)}, f32[3,128,16,64]{1,0,3,2:T(4,128)}, u32[]{:S(2)}) copy-start(f32[3,128,16,64]{1,0,3,2:T(4,128)} %mul.177) | copy-start | bytes 4718596
  42.8 5.6 %copy-start.14 = (f32[3,128,16,64]{1,0,3,2:T(4,128)S(1)}, f32[3,128,16,64]{1,0,3,2:T(4,128)}, u32[]{:S(2)}) copy-start(f32[3,128,16,64]{1,0,3,2:T(4,128)} %mul.179) | copy-start | bytes 4718596
  42.8 5.7 %copy-start.15 = (bf16[16,128,128]{2,1,0:T(8,128)(2,1)S(1)}, bf16[16,128,128]{2,1,0:T(8,128)(2,1)}, u32[]{:S(2)}) copy-start(bf16[16,128,128]{2,1,0:T(8,128)(2,1)} %param.18) | copy-start | bytes 1572868
  48.5 4.1 copy-start.11
  48.5 5.2 %copy-start.19 = (f32[16,128]{1,0:T(8,128)S(1)}, f32[16,128]{1,0:T(8,128)}, u32[]{:S(2)}) copy-start(f32[16,128]{1,0:T(8,128)} %param.19) | copy-start | bytes 24580
  52.6 1.1 copy-start.6
  54.2 1.1 copy-start.4
  54.3 1.4 copy-start.5
  56.4 2.9 copy-start.8
  56.4 1.4 copy-start.3
  59.4 0.9 copy-start.10
  69.6 0.9 copy-start.16
  69.6 1.0 copy-start.17
  69.6 250.7 %all-gather.2.cloned.1.call-start = ((), (), s32[]{:S(2)}) async-start(), calls=%async_computation.1 | async-start | bytes 8912896 | tf_op jit(solution)/shard_map/all_gather | solution.py:82
  71.5 416.0 %all-reduce.3.cloned.1.call-start = ((), (), s32[]{:S(2)}) async-start(), calls=%async_computation.3 | async-start | bytes 2097152 | tf_op jit(solution)/shard_map/psum | solution.py:100
  173.3 24.0 %collective-permute-start = (f32[128,2048]{0,1:T(8,128)}, f32[128,2048]{0,1:T(8,128)S(1)}, u32[]{:S(2)}, u32[]{:S(2)}) collective-permute-start(f32[128,2048]{0,1:T(8,128)} %reduce-scatter.2.cloned.1.call-done), channel_id=1, source_target_pairs={{0,16},{16,0},{32,48},{48,32},{64,80},{80,64},{96,112},{112,96},{1... | collective-permute-start | bytes 3145736 | tf_op jit(solution)/shard_map/ppermute | solution.py:97
  198.7 26.6 %copy-start.7 = (f32[3,128,16,64]{1,3,0,2:T(8,128)S(1)}, f32[3,128,16,64]{1,3,0,2:T(8,128)}, u32[]{:S(2)}) copy-start(f32[3,128,16,64]{1,3,0,2:T(8,128)} %copy-done.6) | copy-start | bytes 4718596
  198.7 26.6 %copy-start.12 = (bf16[3,128,16,64]{1,3,0,2:T(8,128)(2,1)S(1)}, bf16[3,128,16,64]{1,3,0,2:T(8,128)(2,1)}, u32[]{:S(2)}) copy-start(bf16[3,128,16,64]{1,3,0,2:T(8,128)(2,1)} %copy-done.11) | copy-start | bytes 2359300
  198.7 24.9 %collective-permute-start.1 = (f32[128,2048]{0,1:T(8,128)S(1)}, f32[128,2048]{0,1:T(8,128)S(1)}, u32[]{:S(2)}, u32[]{:S(2)}) collective-permute-start(f32[128,2048]{0,1:T(8,128)S(1)} %add.77), channel_id=1, source_target_pairs={{0,32},{16,48},{32,0},{48,16},{64,96},{80,112},{96,64},{112,80},{1... | collective-permute-start | bytes 3145736 | tf_op jit(solution)/shard_map/ppermute | solution.py:97
  223.7 93.0 %collective-permute-start.2 = (f32[128,2048]{0,1:T(8,128)S(1)}, f32[128,2048]{0,1:T(8,128)}, u32[]{:S(2)}, u32[]{:S(2)}) collective-permute-start(f32[128,2048]{0,1:T(8,128)S(1)} %add.78), channel_id=1, source_target_pairs={{0,64},{16,80},{32,96},{48,112},{64,0},{80,16},{96,32},{112,48},{1... | collective-permute-start | bytes 3145736 | tf_op jit(solution)/shard_map/ppermute | solution.py:97
  316.7 3.6 copy-start.9
  318.1 26.1 %collective-permute-start.3 = (f32[128,2048]{0,1:T(8,128)S(1)}, f32[128,2048]{0,1:T(8,128)S(1)}, u32[]{:S(2)}, u32[]{:S(2)}) collective-permute-start(f32[128,2048]{0,1:T(8,128)S(1)} %add.79), channel_id=1, source_target_pairs={{0,128},{16,144},{32,160},{48,176},{64,192},{80,208},{96,224},{112... | collective-permute-start | bytes 3145736 | tf_op jit(solution)/shard_map/ppermute | solution.py:97
  345.4 144.4 %copy-start.1 = (bf16[1,384,2048]{2,1,0:T(8,128)(2,1)S(1)}, bf16[1,384,2048]{2,1,0:T(8,128)(2,1)}, u32[]{:S(2)}) copy-start(bf16[1,384,2048]{2,1,0:T(8,128)(2,1)} %param.10) | copy-start | bytes 4718596
Sparse Core Ops, SparseCore 0:
  69.8 103.4 reduce-scatter.1
  175.7 54.7 all-gather.1
Sparse Core Ops, SparseCore 1:
  227.2 260.2 all-reduce.2
